TPU v7x, 512 devices: a whole 4x8x8 slice. The times are simulated.
512 devices in a mesh: ep: 32 (over z, x), tp: 16 (over y, core).
Axes of the slice: x: 4, y: 8, z: 8, core: 2. Of those that a mesh axis runs over, the one named last changes fastest.
Arguments:
- mix_input: bfloat16 [16384, 2048], P('ep', 'tp'), may hold values from -6 to 6
- mix_weight: bfloat16 [2048, 4096], P(None, 'tp'), may hold values from -0.125 to 0.125
- expert_input: bfloat16 [4096, 4096], P('ep', 'tp'), may hold values from -4500 to 4500
- expert_index: int32 [4096, 2], P('ep'), may hold values from 0 to 31, as said below
- route_share: float32 [4096, 2], P('ep'), may hold values from 0.1 to 1
- norm_gain: float32 [4096], replicated, may hold values from 0.1 to 1.9
- gate_weight: bfloat16 [32, 4096, 2048], P('ep', None, 'tp'), may hold values from -0.09375 to 0.09375
- up_weight: bfloat16 [32, 4096, 2048], P('ep', None, 'tp'), may hold values from -0.09375 to 0.09375
- down_weight: bfloat16 [32, 2048, 4096], P('ep', None, 'tp'), may hold values from -0.125 to 0.125
Outputs:
- mixed_rows: bfloat16 [16384, 4096], P('ep', 'tp')
- expert_rows: bfloat16 [4096, 4096], P('ep', 'tp')
Inputs may be any that keep to these rules, and one draw needn't show every extreme that they name: `expert_index`: each row names 2 different experts. Within each aligned block of 128 rows (the rows of one index of ep) no expert is named by more than 16 rows, and one expert, the same in every block, is named by exactly 16 rows.
All inputs are finite; a program needn't handle non-finite values.
Results may differ from a plain program's by a relative error of at most 0.007.
Values may be sent and summed in bfloat16 or wider, within the bound.
No kernel may reach another device: no remote copies, remote signals or barrier semaphores. Data moves between devices by JAX's collectives and lax.ppermute only.
A program may use at most 64 MiB of HBM per device.

v0:
```python
import jax
import jax.numpy as jnp
from jax import lax
from jax.sharding import PartitionSpec as P

POOL = 2048
TOP = 2
window_reach = 15
norm_eps = 1e-06


def passed_along(value, axis, by):
    size = lax.axis_size(axis)
    pairs = [(i, i + by) for i in range(size) if 0 <= i + by < size]
    return lax.ppermute(value, axis, pairs)


def laid_out(parts, dim):
    lengths = list(parts.shape[1:])
    lengths[dim] *= parts.shape[0]
    return jnp.moveaxis(parts, 0, dim).reshape(lengths)


def copy_for_each(value, axis):
    size = lax.axis_size(axis)
    return lax.all_to_all(
        jnp.broadcast_to(value[None], (size, *value.shape)), axis, 0, 0, tiled=True
    )


def gathered_copies(value, axis, dim):
    return laid_out(copy_for_each(value, axis), dim)


def pool_minus_self(extended, first_pos, group_size, channel_base):
    length = extended.shape[0] - window_reach
    channels = extended.shape[1]
    channel = channel_base + jnp.arange(channels, dtype=jnp.int32)
    window = jnp.power(2, channel // group_size + 1).astype(jnp.int32)
    running = jnp.zeros((length, channels), jnp.float32)
    for lag_count in range(window_reach + 1):
        shifted = extended[window_reach - lag_count : window_reach - lag_count + length]
        running = running + jnp.where(lag_count < window[None, :], shifted, 0.0)
    position = first_pos + jnp.arange(length, dtype=jnp.int32)
    counts = jnp.minimum(position[:, None] + 1, window[None, :]).astype(jnp.float32)
    return (running / counts - extended[window_reach:]).astype(jnp.bfloat16)


def slot_targets(indices, experts, capacity):
    flattened = indices.reshape(-1)
    one_hot = (flattened[:, None] == jnp.arange(experts, dtype=jnp.int32)[None, :]).astype(
        jnp.int32
    )
    earlier = jnp.cumsum(one_hot, axis=0) - one_hot
    return flattened * capacity + jnp.sum(earlier * one_hot, axis=1)


def shards(
    mix_input,
    mix_weight,
    expert_input,
    expert_index,
    route_share,
    norm_gain,
    gate_weight,
    up_weight,
    down_weight,
):
    tokens_mix, channels = mix_input.shape
    trailing = mix_input[tokens_mix - window_reach :]
    previous = passed_along(trailing, "ep", 1)
    extended = jnp.concatenate([previous, mix_input], axis=0).astype(jnp.float32)
    pooled = pool_minus_self(
        extended, lax.axis_index("ep") * tokens_mix, POOL // 4, lax.axis_index("tp") * channels
    )
    mixed_rows = jnp.dot(
        lax.all_gather(pooled, "tp", axis=1, tiled=True),
        mix_weight,
        preferred_element_type=jnp.float32,
    ).astype(jnp.bfloat16)
    tokens_exp = expert_input.shape[0]
    local_experts = gate_weight.shape[0]
    experts = local_experts * lax.axis_size("ep")
    capacity = 2 * tokens_exp * TOP // experts
    model_width = norm_gain.shape[0]
    targets = slot_targets(expert_index, experts, capacity)
    sources = jnp.repeat(jnp.arange(tokens_exp, dtype=jnp.int32), TOP)
    table = jnp.full((experts * capacity,), tokens_exp, jnp.int32).at[targets].set(sources)
    feature_block = expert_input.shape[1]
    padded = jnp.concatenate([expert_input, jnp.zeros((1, feature_block), jnp.bfloat16)], axis=0)
    outgoing = padded[table].reshape(experts, capacity, feature_block)
    arrived = lax.all_to_all(outgoing, "ep", split_axis=0, concat_axis=1, tiled=True)
    portion = lax.all_gather(arrived, "tp", axis=2, tiled=True)
    scaled = (portion.astype(jnp.float32) * norm_gain).astype(jnp.bfloat16)
    gate_acts = jnp.einsum("erd,edh->erh", scaled, gate_weight, preferred_element_type=jnp.float32)
    up_acts = jnp.einsum("erd,edh->erh", scaled, up_weight, preferred_element_type=jnp.float32)
    squares = jnp.sum(jnp.square(portion.astype(jnp.float32)), axis=2)
    inverse = lax.rsqrt(squares / model_width + norm_eps)[:, :, None]
    hidden = (jax.nn.silu(gate_acts * inverse) * (up_acts * inverse)).astype(jnp.bfloat16)
    produced = jnp.einsum(
        "erh,ehc->erc",
        gathered_copies(hidden, "tp", 2),
        down_weight,
        preferred_element_type=jnp.float32,
    ).astype(jnp.bfloat16)
    returned = lax.all_to_all(produced, "ep", split_axis=1, concat_axis=0, tiled=True)
    returned = returned.reshape(experts * capacity, returned.shape[2])
    picked = returned[targets].astype(jnp.float32).reshape(tokens_exp, TOP, returned.shape[1])
    shares = route_share / jnp.sum(route_share, axis=1, keepdims=True)
    expert_rows = jnp.sum(picked * shares[:, :, None], axis=1).astype(jnp.bfloat16)
    return (mixed_rows, expert_rows)


def solution(mesh):
    placed = (
        P("ep", "tp"),
        P(None, "tp"),
        P("ep", "tp"),
        P("ep", None),
        P("ep", None),
        P(),
        P("ep", None, "tp"),
        P("ep", None, "tp"),
        P("ep", None, "tp"),
    )
    return jax.shard_map(
        shards,
        mesh=mesh,
        in_specs=placed,
        out_specs=(P("ep", "tp"), P("ep", "tp")),
        check_vma=False,
    )
```

profile of v0, /device:TPU:24, one launch (start us, length us, event | category | flops | bytes accessed | tf_op | source)
XLA Modules:
  0.0 192.1 jit_solution(15322384750593228259)
XLA Ops:
  7.2 0.0 copy-start
  7.2 0.0 all-gather.5.cloned.1.call-start
  7.2 0.8 broadcast_multiply_fusion
  8.1 0.8 copy.27
  8.8 0.1 eq.29
  9.0 0.1 eq.25
  9.1 0.1 copy.26
  9.2 0.1 mul.314
  9.4 0.6 reduce-window.6
  10.0 0.2 slice_reduce_fusion
  10.2 0.1 reshape.270
  10.4 0.1 fusion.43
  10.5 1.4 scatter_custom_fusion
  11.9 0.8 concatenate.7
  12.8 1.9 %gather_fusion = bf16[512,256]{1,0:T(8,128)(2,1)S(1)} fusion(bf16[129,256]{1,0:T(8,128)(2,1)S(1)} %concatenate.7, s32[1024]{0:T(1024)S(1)} %pad_clamp_fusion.1), kind=kCustom, calls=%fused_computation | custom fusion | bytes 526336 | tf_op jit(solution)/shard_map/gather | solution.py:91
  14.7 25.9 %all_to_all.26 = bf16[32,16,256]{2,1,0:T(8,128)(2,1)} all-to-all(bf16[32,16,256]{2,1,0:T(8,128)(2,1)S(1)} %bitcast.67), channel_id=1, replica_groups=mesh['ep'=32,'tp'=16] {'ep'}, dimensions={0} | all-to-all | bytes 524288 | tf_op jit(solution)/shard_map/all_to_all | solution.py:92
  40.6 0.0 all-gather.5.cloned.1.call-update
  40.6 0.7 slice.58
  41.3 2.1 %collective-permute-start = (bf16[15,128]{1,0:T(8,128)(2,1)S(1)}, bf16[15,128]{1,0:T(8,128)(2,1)S(1)}, u32[]{:S(2)}, u32[]{:S(2)}) collective-permute-start(bf16[15,128]{1,0:T(8,128)(2,1)S(1)} %slice.58), channel_id=1, source_target_pairs={{0,16},{16,32},{32,48},{48,64},{64,80},{80,96},{96,112},{112,128},... | collective-permute-start | bytes 11528 | tf_op jit(solution)/shard_map/ppermute | solution.py:15
  43.6 42.6 %all-gather.5.cloned.1.call-done = bf16[1,512,4096]{2,1,0:T(8,128)(2,1)} async-done(((bf16[1,512,256]{2,1,0:T(8,128)(2,1)}), bf16[1,512,4096]{2,1,0:T(8,128)(2,1)}) %all-gather.5.cloned.1.call-update) | async-done | bytes 4194320 | tf_op jit(solution)/shard_map/all_gather | solution.py:93
  86.2 3.2 %fusion.1 = f32[512]{0:T(512)S(1)} fusion(bf16[1,512,4096]{2,1,0:T(8,128)(2,1)} %all-gather.5.cloned.1.call-done), kind=kLoop, calls=%fused_computation.6 | loop fusion | flops 6290944 | bytes 4196352 | tf_op jit(solution)/shard_map/reduce_sum | solution.py:97
  89.4 0.2 copy-done.1
  89.6 1.3 fusion.8
  90.9 0.0 copy-done.5
  90.9 1.3 fusion.17
  92.2 0.0 copy-start.2
  92.2 0.1 copy.30
  92.3 1.5 broadcast_in_dim.167
  93.8 6.5 %all-to-all-start.1 = ((bf16[16,1,512,128]{2,3,1,0:T(8,128)(2,1)}), bf16[16,1,512,128]{2,3,1,0:T(8,128)(2,1)S(1)}, u32[]{:S(2)}, u32[]{:S(2)}) async-start(bf16[16,1,512,128]{2,3,1,0:T(8,128)(2,1)} %broadcast_in_dim.167), calls=%async_computation.1 | async-start | bytes 4194304 | tf_op jit(solution)/shard_map/all_to_all | solution.py:26
  100.3 0.0 all-gather.3.cloned.1.call-start
  100.4 0.0 collective-permute-done
  100.4 1.2 fusion.40
  101.7 0.0 all-gather.3.cloned.1.call-update
  101.7 52.9 %all-to-all-done.1 = bf16[16,1,512,128]{2,3,1,0:T(8,128)(2,1)S(1)} async-done(((bf16[16,1,512,128]{2,3,1,0:T(8,128)(2,1)}), bf16[16,1,512,128]{2,3,1,0:T(8,128)(2,1)S(1)}, u32[]{:S(2)}, u32[]{:S(2)}) %all-to-all-start.1) | async-done | bytes 2097184 | tf_op jit(solution)/shard_map/all_to_all | solution.py:26
  154.6 0.8 fusion.7
  155.4 0.4 copy.40
  155.8 0.5 broadcast.1945
  156.3 2.3 %reduce.3 = bf16[512,256]{1,0:T(8,128)(2,1)S(1)} reduce(bf16[512,1,256]{2,1,0:T(2,128)(2,1)S(1)} %bitcast.65, bf16[]{:T(256)} %broadcast.1945), dimensions={1}, to_apply=%bitcast.60.reduce_sub_computation | reduce | bytes 524290
  158.6 0.8 reshape.278
  159.4 10.0 %all-to-all-start.2 = ((bf16[32,2,2048]{2,1,0:T(2,128)(2,1)}), bf16[32,2,2048]{2,1,0:T(2,128)(2,1)S(1)}, u32[]{:S(2)}, u32[]{:S(2)}) async-start(bf16[32,2,2048]{2,1,0:T(2,128)(2,1)} %reshape.278), calls=%async_computation.2 | async-start | bytes 524288 | tf_op jit(solution)/shard_map/all_to_all | solution.py:106
  169.4 0.1 copy.33
  169.5 0.0 all-gather.3.cloned.1.call-done
  169.5 3.3 %convolution_convert_fusion.1 = bf16[512,256]{1,0:T(8,128)(2,1)} fusion(bf16[512,2048]{1,0:T(8,128)(2,1)} %all-gather.3.cloned.1.call-done, bf16[2048,256]{1,0:T(8,128)(2,1)} %param.10), kind=kOutput, calls=%fused_computation.11 | convolution fusion | flops 537001984 | bytes 3407872 | tf_op jit(solution)/shard_map/dot_general | solution.py:76
  172.8 9.8 %all-to-all-done.2 = bf16[32,2,2048]{2,1,0:T(2,128)(2,1)S(1)} async-done(((bf16[32,2,2048]{2,1,0:T(2,128)(2,1)}), bf16[32,2,2048]{2,1,0:T(2,128)(2,1)S(1)}, u32[]{:S(2)}, u32[]{:S(2)}) %all-to-all-start.2) | async-done | bytes 262176 | tf_op jit(solution)/shard_map/all_to_all | solution.py:106
  182.6 0.3 reshape.279
  182.9 1.2 gather_fusion.1
  184.1 0.1 reshape.249
  184.2 1.0 multiply_reduce_fusion
  (33 shorter events, 0.4 us)
Async XLA Ops:
  7.2 147.4 %copy-start = (bf16[1,2048,256]{2,1,0:T(8,128)(2,1)S(1)}, bf16[1,2048,256]{2,1,0:T(8,128)(2,1)}, u32[]{:S(2)}) copy-start(bf16[1,2048,256]{2,1,0:T(8,128)(2,1)} %param.17) | copy-start | bytes 3145732
  7.2 82.2 %copy-start.6 = (f32[4096]{0:T(1024)S(1)}, f32[4096]{0:T(1024)}, u32[]{:S(2)}) copy-start(f32[4096]{0:T(1024)} %param.14) | copy-start | bytes 49156
  7.2 82.2 %copy-start.4 = (bf16[1,4096,128]{2,1,0:T(8,128)(2,1)S(1)}, bf16[1,4096,128]{2,1,0:T(8,128)(2,1)}, u32[]{:S(2)}) copy-start(bf16[1,4096,128]{2,1,0:T(8,128)(2,1)} %param.15) | copy-start | bytes 3145732
  7.2 79.0 %all-gather.5.cloned.1.call-start = ((), (), s32[]{:S(2)}) async-start(), calls=%async_computation.4 | async-start | bytes 4456448 | tf_op jit(solution)/shard_map/all_gather | solution.py:93
  41.3 59.1 %collective-permute-start = (bf16[15,128]{1,0:T(8,128)(2,1)S(1)}, bf16[15,128]{1,0:T(8,128)(2,1)S(1)}, u32[]{:S(2)}, u32[]{:S(2)}) collective-permute-start(bf16[15,128]{1,0:T(8,128)(2,1)S(1)} %slice.58), channel_id=1, source_target_pairs={{0,16},{16,32},{32,48},{48,64},{64,80},{80,96},{96,112},{112,128},... | collective-permute-start | bytes 11528 | tf_op jit(solution)/shard_map/ppermute | solution.py:15
  86.2 3.4 %copy-start.1 = (bf16[1,512,4096]{2,1,0:T(8,128)(2,1)S(1)}, bf16[1,512,4096]{2,1,0:T(8,128)(2,1)}, u32[]{:S(2)}) copy-start(bf16[1,512,4096]{2,1,0:T(8,128)(2,1)} %all-gather.5.cloned.1.call-done) | copy-start | bytes 12582916
  89.4 1.5 copy-start.5
  92.2 8.2 %copy-start.2 = (bf16[512,128]{1,0:T(8,128)(2,1)S(1)}, bf16[512,128]{1,0:T(8,128)(2,1)}, u32[]{:S(2)}) copy-start(bf16[512,128]{1,0:T(8,128)(2,1)} %param.9) | copy-start | bytes 393220
  93.8 7.9 %copy-start.3 = (f32[128,2]{0,1:T(2,128)S(1)}, f32[128,2]{0,1:T(2,128)}, u32[]{:S(2)}) copy-start(f32[128,2]{0,1:T(2,128)} %param.13) | copy-start | bytes 3076
  93.8 60.8 %all-to-all-start.1 = ((bf16[16,1,512,128]{2,3,1,0:T(8,128)(2,1)}), bf16[16,1,512,128]{2,3,1,0:T(8,128)(2,1)S(1)}, u32[]{:S(2)}, u32[]{:S(2)}) async-start(bf16[16,1,512,128]{2,3,1,0:T(8,128)(2,1)} %broadcast_in_dim.167), calls=%async_computation.1 | async-start | bytes 4194304 | tf_op jit(solution)/shard_map/all_to_all | solution.py:26
  100.3 69.2 %all-gather.3.cloned.1.call-start = ((), (), s32[]{:S(2)}) async-start(), calls=%async_computation.3 | async-start | bytes 2228224 | tf_op jit(solution)/shard_map/all_gather | solution.py:77
  159.4 23.2 %all-to-all-start.2 = ((bf16[32,2,2048]{2,1,0:T(2,128)(2,1)}), bf16[32,2,2048]{2,1,0:T(2,128)(2,1)S(1)}, u32[]{:S(2)}, u32[]{:S(2)}) async-start(bf16[32,2,2048]{2,1,0:T(2,128)(2,1)} %reshape.278), calls=%async_computation.2 | async-start | bytes 524288 | tf_op jit(solution)/shard_map/all_to_all | solution.py:106
Sparse Core Ops, SparseCore 0:
  40.7 45.3 all-gather.4
  103.7 61.7 all-gather.2
where the time goes:
time: 192 us
  waiting for transfers between devices  105 us (55%)
  blocking collectives  25.9 us (13%)
  starting transfers between devices  18.6 us (10%)
  between operations  14.3 us (7%)
  local copies, waits for them, and re-layouts  11.8 us (6%)
  other arithmetic  9.6 us (5%)
  matrix products  6.54 us (3%)
    all_to_all x1, waiting for transfers between devices, copy_for_each(): lax.all_to_all(jnp.broadcast_to(value[None], (size, *value.shape)), axis,...  52.9 us
    all_gather x1, waiting for transfers between devices, shards(): portion = lax.all_gather(arrived, 'tp', axis=2, tiled=True)  42.6 us
    all_to_all x1, blocking collectives, shards(): lax.all_to_all(outgoing, 'ep', split_axis=0, concat_axis=1, tiled=True)  25.9 us
    all_to_all x1, starting transfers between devices, shards(): lax.all_to_all(produced, 'ep', split_axis=1, concat_axis=0, tiled=True)  9.99 us
    all_to_all x1, waiting for transfers between devices, shards(): lax.all_to_all(produced, 'ep', split_axis=1, concat_axis=0, tiled=True)  9.79 us
    all_to_all x1, starting transfers between devices, copy_for_each(): lax.all_to_all(jnp.broadcast_to(value[None], (size, *value.shape)), axis,...  6.49 us
  transfers between devices with their start and end apart: 5, of which 3 were waited for; matrix products, arithmetic and copies ran while one was open for 9% of the time, Pallas kernels for 0%

commit v1 on v0

--- a/solution.py
+++ b/solution.py
@@ -90,7 +90,24 @@
     padded = jnp.concatenate([expert_input, jnp.zeros((1, feature_block), jnp.bfloat16)], axis=0)
     outgoing = padded[table].reshape(experts, capacity, feature_block)
     arrived = lax.all_to_all(outgoing, "ep", split_axis=0, concat_axis=1, tiled=True)
-    portion = lax.all_gather(arrived, "tp", axis=2, tiled=True)
+    size_2, place, extent = (lax.axis_size("tp"), lax.axis_index("tp"), arrived.shape[2])
+    forward = [(i_2, (i_2 + 1) % size_2) for i_2 in range(size_2)]
+    left = [(i_2, (i_2 - 1) % size_2) for i_2 in range(size_2)]
+    out = jnp.zeros((*arrived.shape[:2], size_2 * extent, *arrived.shape[2 + 1 :]), arrived.dtype)
+    out = lax.dynamic_update_slice_in_dim(out, arrived, place * extent, axis=2)
+    from_left = from_right = arrived
+    middle = size_2 // 2
+    for step in range(1, middle + 1):
+        from_left = lax.ppermute(from_left, "tp", forward)
+        out = lax.dynamic_update_slice_in_dim(
+            out, from_left, (place - step) % size_2 * extent, axis=2
+        )
+        if step < size_2 - middle:
+            from_right = lax.ppermute(from_right, "tp", left)
+            out = lax.dynamic_update_slice_in_dim(
+                out, from_right, (place + step) % size_2 * extent, axis=2
+            )
+    portion = out
     scaled = (portion.astype(jnp.float32) * norm_gain).astype(jnp.bfloat16)
     gate_acts = jnp.einsum("erd,edh->erh", scaled, gate_weight, preferred_element_type=jnp.float32)
     up_acts = jnp.einsum("erd,edh->erh", scaled, up_weight, preferred_element_type=jnp.float32)

time: 192 us -> 196 us (1.021)
  starting transfers between devices: 18.6 us -> 56.5 us
  waiting for transfers between devices: 105 us -> 72.7 us
  other arithmetic: 9.6 us -> 7.06 us
    all_gather x1 -> x0, waiting for transfers between devices: 42.6 us -> none  [shards(): portion = lax.all_gather(arrived, 'tp', axis=2, tiled=True)]
    ppermute x0 -> x15, starting transfers between devices: none -> 34.9 us  [the longest x8 25.9 us: shards(): from_left = lax.ppermute(from_left, 'tp', forward)]
    ppermute x0 -> x15, waiting for transfers between devices: none -> 10.2 us  [the longest x8 6.49 us: shards(): from_left = lax.ppermute(from_left, 'tp', forward)]
    all_to_all x1, starting transfers between devices: 6.49 us -> 14.1 us  [copy_for_each(): lax.all_to_all(jnp.broadcast_to(value[None], (size, *value.shape)), axis,...]
    all_to_all x1, starting transfers between devices: 9.99 us -> 5.15 us  [shards(): lax.all_to_all(produced, 'ep', split_axis=1, concat_axis=0, tiled=True)]
    reduce_sum x1, other arithmetic: 3.23 us -> 0.9 us  [shards(): squares = jnp.sum(jnp.square(portion.astype(jnp.float32)), axis=2)]
    all_gather x1, waiting for transfers between devices: 0.02 us -> 2.28 us  [shards(): lax.all_gather(pooled, 'tp', axis=1, tiled=True)]
    all_to_all x1, waiting for transfers between devices: 9.79 us -> 7.54 us  [shards(): lax.all_to_all(produced, 'ep', split_axis=1, concat_axis=0, tiled=True)]
  transfers between devices with their start and end apart: 5 -> 19, of which waited for: 3 -> 17; matrix products, arithmetic and copies ran while one was open for 9% -> 8% of each run, Pallas kernels for 0% -> 0%
where the time goes in v1:
time: 196 us
  waiting for transfers between devices  72.7 us (37%)
  starting transfers between devices  56.5 us (29%)
  blocking collectives  25.8 us (13%)
  between operations  14.8 us (8%)
  local copies, waits for them, and re-layouts  12.6 us (6%)
  other arithmetic  7.06 us (4%)
  matrix products  6.56 us (3%)
    all_to_all x1, waiting for transfers between devices, copy_for_each(): lax.all_to_all(jnp.broadcast_to(value[None], (size, *value.shape)), axis,...  52.7 us
    ppermute x8, starting transfers between devices, shards(): from_left = lax.ppermute(from_left, 'tp', forward)  25.9 us
    all_to_all x1, blocking collectives, shards(): lax.all_to_all(outgoing, 'ep', split_axis=0, concat_axis=1, tiled=True)  25.8 us
    all_to_all x1, starting transfers between devices, copy_for_each(): lax.all_to_all(jnp.broadcast_to(value[None], (size, *value.shape)), axis,...  14.1 us
    ppermute x7, starting transfers between devices, shards(): from_right = lax.ppermute(from_right, 'tp', left)  9.03 us
    all_to_all x1, waiting for transfers between devices, shards(): lax.all_to_all(produced, 'ep', split_axis=1, concat_axis=0, tiled=True)  7.54 us
    ppermute x8, waiting for transfers between devices, shards(): from_left = lax.ppermute(from_left, 'tp', forward)  6.49 us
    all_to_all x1, starting transfers between devices, shards(): lax.all_to_all(produced, 'ep', split_axis=1, concat_axis=0, tiled=True)  5.15 us
  transfers between devices with their start and end apart: 19, of which 17 were waited for; matrix products, arithmetic and copies ran while one was open for 8% of the time, Pallas kernels for 0%

profile of v1, /device:TPU:24, one launch (start us, length us, event | category | flops | bytes accessed | tf_op | source)
XLA Modules:
  0.0 195.9 jit_solution(11184812887582910)
XLA Ops:
  7.2 0.9 copy.27
  8.3 0.7 broadcast_multiply_fusion
  9.0 0.6 reduce-window.6
  10.4 1.4 scatter_custom_fusion
  11.8 0.8 concatenate.7
  12.6 1.9 gather_fusion
  14.6 25.8 %all_to_all.26 = bf16[32,16,256]{2,1,0:T(8,128)(2,1)S(1)} all-to-all(bf16[32,16,256]{2,1,0:T(8,128)(2,1)S(1)} %bitcast.70), channel_id=1, replica_groups=mesh['ep'=32,'tp'=16] {'ep'}, dimensions={0} | all-to-all | bytes 524288 | tf_op jit(solution)/shard_map/all_to_all | solution.py:92
  40.4 0.7 slice.58
  41.1 2.1 %collective-permute-start = (bf16[15,128]{1,0:T(8,128)(2,1)S(1)}, bf16[15,128]{1,0:T(8,128)(2,1)S(1)}, u32[]{:S(2)}, u32[]{:S(2)}) collective-permute-start(bf16[15,128]{1,0:T(8,128)(2,1)S(1)} %slice.58), channel_id=1, source_target_pairs={{0,16},{16,32},{32,48},{48,64},{64,80},{80,96},{96,112},{112,128},... | collective-permute-start | bytes 11528 | tf_op jit(solution)/shard_map/ppermute | solution.py:15
  43.2 1.5 collective-permute-start.2
  44.7 1.5 collective-permute-done.1
  46.2 0.4 collective-permute-start.3
  46.6 1.9 collective-permute-done.2
  48.6 2.2 %collective-permute-start.4 = (bf16[1,512,256]{2,1,0:T(8,128)(2,1)S(1)}, bf16[1,512,256]{2,1,0:T(8,128)(2,1)S(1)}, u32[]{:S(2)}, u32[]{:S(2)}) collective-permute-start(bf16[1,512,256]{2,1,0:T(8,128)(2,1)S(1)} %collective-permute-done.2), channel_id=1, source_target_pairs={{0,15},{1,0},{2,1},{3,2},{4,3},{5,4},{6,5},{7,6},{8,7},{9,8},{10,9... | collective-permute-start | bytes 786440 | tf_op jit(solution)/shard_map/ppermute | solution.py:106
  50.8 1.2 collective-permute-done.3
  52.0 1.6 collective-permute-start.5
  53.6 1.0 collective-permute-done.4
  54.7 2.2 %collective-permute-start.6 = (bf16[1,512,256]{2,1,0:T(8,128)(2,1)S(1)}, bf16[1,512,256]{2,1,0:T(8,128)(2,1)S(1)}, u32[]{:S(2)}, u32[]{:S(2)}) collective-permute-start(bf16[1,512,256]{2,1,0:T(8,128)(2,1)S(1)} %collective-permute-done.4), channel_id=1, source_target_pairs={{0,15},{1,0},{2,1},{3,2},{4,3},{5,4},{6,5},{7,6},{8,7},{9,8},{10,9... | collective-permute-start | bytes 786440 | tf_op jit(solution)/shard_map/ppermute | solution.py:106
  57.2 0.6 collective-permute-done.5
  57.8 2.8 %collective-permute-start.7 = (bf16[1,512,256]{2,1,0:T(8,128)(2,1)S(1)}, bf16[1,512,256]{2,1,0:T(8,128)(2,1)S(1)}, u32[]{:S(2)}, u32[]{:S(2)}) collective-permute-start(bf16[1,512,256]{2,1,0:T(8,128)(2,1)S(1)} %collective-permute-done.5), channel_id=1, source_target_pairs={{0,1},{1,2},{2,3},{3,4},{4,5},{5,6},{6,7},{7,8},{8,9},{9,10},{10,1... | collective-permute-start | bytes 786440 | tf_op jit(solution)/shard_map/ppermute | solution.py:101
  60.6 0.5 broadcast_in_dim.167
  61.2 1.7 collective-permute-start.8
  63.0 0.6 collective-permute-done.7
  63.6 4.1 %collective-permute-start.9 = (bf16[1,512,256]{2,1,0:T(8,128)(2,1)S(1)}, bf16[1,512,256]{2,1,0:T(8,128)(2,1)S(1)}, u32[]{:S(2)}, u32[]{:S(2)}) collective-permute-start(bf16[1,512,256]{2,1,0:T(8,128)(2,1)S(1)} %collective-permute-done.7), channel_id=1, source_target_pairs={{0,1},{1,2},{2,3},{3,4},{4,5},{5,6},{6,7},{7,8},{8,9},{9,10},{10,1... | collective-permute-start | bytes 786440 | tf_op jit(solution)/shard_map/ppermute | solution.py:101
  67.9 1.2 collective-permute-start.10
  69.4 5.3 %collective-permute-start.11 = (bf16[1,512,256]{2,1,0:T(8,128)(2,1)S(1)}, bf16[1,512,256]{2,1,0:T(8,128)(2,1)S(1)}, u32[]{:S(2)}, u32[]{:S(2)}) collective-permute-start(bf16[1,512,256]{2,1,0:T(8,128)(2,1)S(1)} %collective-permute-done.9), channel_id=1, source_target_pairs={{0,1},{1,2},{2,3},{3,4},{4,5},{5,6},{6,7},{7,8},{8,9},{9,10},{10,1... | collective-permute-start | bytes 786440 | tf_op jit(solution)/shard_map/ppermute | solution.py:101
  75.2 0.6 collective-permute-done.11
  75.8 5.8 %collective-permute-start.13 = (bf16[1,512,256]{2,1,0:T(8,128)(2,1)S(1)}, bf16[1,512,256]{2,1,0:T(8,128)(2,1)S(1)}, u32[]{:S(2)}, u32[]{:S(2)}) collective-permute-start(bf16[1,512,256]{2,1,0:T(8,128)(2,1)S(1)} %collective-permute-done.11), channel_id=1, source_target_pairs={{0,1},{1,2},{2,3},{3,4},{4,5},{5,6},{6,7},{7,8},{8,9},{9,10},{10,1... | collective-permute-start | bytes 786440 | tf_op jit(solution)/shard_map/ppermute | solution.py:101
  81.9 0.9 collective-permute-done.13
  82.8 5.8 %collective-permute-start.15 = (bf16[1,512,256]{2,1,0:T(8,128)(2,1)S(1)}, bf16[1,512,256]{2,1,0:T(8,128)(2,1)S(1)}, u32[]{:S(2)}, u32[]{:S(2)}) collective-permute-start(bf16[1,512,256]{2,1,0:T(8,128)(2,1)S(1)} %collective-permute-done.13), channel_id=1, source_target_pairs={{0,1},{1,2},{2,3},{3,4},{4,5},{5,6},{6,7},{7,8},{8,9},{9,10},{10,1... | collective-permute-start | bytes 786440 | tf_op jit(solution)/shard_map/ppermute | solution.py:101
  88.9 0.9 collective-permute-done.15
  89.8 0.9 fusion.1
  90.8 1.3 fusion.8
  92.1 1.3 multiply_convert_fusion
  93.5 1.5 broadcast_in_dim.171
  95.0 14.1 %all-to-all-start.1 = ((bf16[16,1,512,128]{2,3,1,0:T(8,128)(2,1)}), bf16[16,1,512,128]{2,3,1,0:T(8,128)(2,1)S(1)}, u32[]{:S(2)}, u32[]{:S(2)}) async-start(bf16[16,1,512,128]{2,3,1,0:T(8,128)(2,1)} %broadcast_in_dim.171), calls=%async_computation.1 | async-start | bytes 4194304 | tf_op jit(solution)/shard_map/all_to_all | solution.py:26
  109.4 1.2 fusion.34
  110.7 52.7 %all-to-all-done.1 = bf16[16,1,512,128]{2,3,1,0:T(8,128)(2,1)S(1)} async-done(((bf16[16,1,512,128]{2,3,1,0:T(8,128)(2,1)}), bf16[16,1,512,128]{2,3,1,0:T(8,128)(2,1)S(1)}, u32[]{:S(2)}, u32[]{:S(2)}) %all-to-all-start.1) | async-done | bytes 2097184 | tf_op jit(solution)/shard_map/all_to_all | solution.py:26
  163.4 0.8 fusion.7
  164.6 0.5 broadcast.1960
  165.1 2.2 %reduce.3 = bf16[512,256]{1,0:T(8,128)(2,1)S(1)} reduce(bf16[512,1,256]{2,1,0:T(2,128)(2,1)S(1)} %bitcast.66, bf16[]{:T(256)} %broadcast.1960), dimensions={1}, to_apply=%bitcast.61.reduce_sub_computation | reduce | bytes 524290
  167.3 0.8 reshape.278
  168.1 5.2 %all-to-all-start.2 = ((bf16[32,2,2048]{2,1,0:T(2,128)(2,1)}), bf16[32,2,2048]{2,1,0:T(2,128)(2,1)S(1)}, u32[]{:S(2)}, u32[]{:S(2)}) async-start(bf16[32,2,2048]{2,1,0:T(2,128)(2,1)} %reshape.278), calls=%async_computation.2 | async-start | bytes 524288 | tf_op jit(solution)/shard_map/all_to_all | solution.py:123
  173.4 2.3 %all-gather.2.cloned.1.call-done = bf16[512,2048]{1,0:T(8,128)(2,1)} async-done(((bf16[512,128]{1,0:T(8,128)(2,1)}), bf16[512,2048]{1,0:T(8,128)(2,1)}) %all-gather.2.cloned.1.call-update) | async-done | bytes 2097168 | tf_op jit(solution)/shard_map/all_gather | solution.py:77
  175.6 3.3 %convolution_convert_fusion.1 = bf16[512,256]{1,0:T(8,128)(2,1)} fusion(bf16[512,2048]{1,0:T(8,128)(2,1)} %all-gather.2.cloned.1.call-done, bf16[2048,256]{1,0:T(8,128)(2,1)} %param.10), kind=kOutput, calls=%fused_computation.11 | convolution fusion | flops 537001984 | bytes 3407872 | tf_op jit(solution)/shard_map/dot_general | solution.py:76
  178.9 7.5 %all-to-all-done.2 = bf16[32,2,2048]{2,1,0:T(2,128)(2,1)S(1)} async-done(((bf16[32,2,2048]{2,1,0:T(2,128)(2,1)}), bf16[32,2,2048]{2,1,0:T(2,128)(2,1)S(1)}, u32[]{:S(2)}, u32[]{:S(2)}) %all-to-all-start.2) | async-done | bytes 262176 | tf_op jit(solution)/shard_map/all_to_all | solution.py:123
  186.8 1.2 gather_fusion.1
  188.1 1.0 multiply_reduce_fusion
  (75 shorter events, 4.3 us)
Async XLA Ops:
  7.2 156.2 %copy-start = (bf16[1,2048,256]{2,1,0:T(8,128)(2,1)S(1)}, bf16[1,2048,256]{2,1,0:T(8,128)(2,1)}, u32[]{:S(2)}) copy-start(bf16[1,2048,256]{2,1,0:T(8,128)(2,1)} %param.17) | copy-start | bytes 3145732
  40.4 5.8 %collective-permute-start.1 = (bf16[1,512,256]{2,1,0:T(8,128)(2,1)S(1)}, bf16[1,512,256]{2,1,0:T(8,128)(2,1)S(1)}, u32[]{:S(2)}, u32[]{:S(2)}) collective-permute-start(bf16[1,512,256]{2,1,0:T(8,128)(2,1)S(1)} %bitcast.67), channel_id=1, source_target_pairs={{0,1},{1,2},{2,3},{3,4},{4,5},{5,6},{6,7},{7,8},{8,9},{9,10},{10,1... | collective-permute-start | bytes 786440 | tf_op jit(solution)/shard_map/ppermute | solution.py:101
  41.1 68.3 %collective-permute-start = (bf16[15,128]{1,0:T(8,128)(2,1)S(1)}, bf16[15,128]{1,0:T(8,128)(2,1)S(1)}, u32[]{:S(2)}, u32[]{:S(2)}) collective-permute-start(bf16[15,128]{1,0:T(8,128)(2,1)S(1)} %slice.58), channel_id=1, source_target_pairs={{0,16},{16,32},{32,48},{48,64},{64,80},{80,96},{96,112},{112,128},... | collective-permute-start | bytes 11528 | tf_op jit(solution)/shard_map/ppermute | solution.py:15
  43.2 5.4 %collective-permute-start.2 = (bf16[1,512,256]{2,1,0:T(8,128)(2,1)S(1)}, bf16[1,512,256]{2,1,0:T(8,128)(2,1)S(1)}, u32[]{:S(2)}, u32[]{:S(2)}) collective-permute-start(bf16[1,512,256]{2,1,0:T(8,128)(2,1)S(1)} %bitcast.68), channel_id=1, source_target_pairs={{0,15},{1,0},{2,1},{3,2},{4,3},{5,4},{6,5},{7,6},{8,7},{9,8},{10,9... | collective-permute-start | bytes 786440 | tf_op jit(solution)/shard_map/ppermute | solution.py:106
  46.2 5.8 %collective-permute-start.3 = (bf16[1,512,256]{2,1,0:T(8,128)(2,1)S(1)}, bf16[1,512,256]{2,1,0:T(8,128)(2,1)S(1)}, u32[]{:S(2)}, u32[]{:S(2)}) collective-permute-start(bf16[1,512,256]{2,1,0:T(8,128)(2,1)S(1)} %collective-permute-done.1), channel_id=1, source_target_pairs={{0,1},{1,2},{2,3},{3,4},{4,5},{5,6},{6,7},{7,8},{8,9},{9,10},{10,1... | collective-permute-start | bytes 786440 | tf_op jit(solution)/shard_map/ppermute | solution.py:101
  48.6 6.1 %collective-permute-start.4 = (bf16[1,512,256]{2,1,0:T(8,128)(2,1)S(1)}, bf16[1,512,256]{2,1,0:T(8,128)(2,1)S(1)}, u32[]{:S(2)}, u32[]{:S(2)}) collective-permute-start(bf16[1,512,256]{2,1,0:T(8,128)(2,1)S(1)} %collective-permute-done.2), channel_id=1, source_target_pairs={{0,15},{1,0},{2,1},{3,2},{4,3},{5,4},{6,5},{7,6},{8,7},{9,8},{10,9... | collective-permute-start | bytes 786440 | tf_op jit(solution)/shard_map/ppermute | solution.py:106
  52.0 5.8 %collective-permute-start.5 = (bf16[1,512,256]{2,1,0:T(8,128)(2,1)S(1)}, bf16[1,512,256]{2,1,0:T(8,128)(2,1)S(1)}, u32[]{:S(2)}, u32[]{:S(2)}) collective-permute-start(bf16[1,512,256]{2,1,0:T(8,128)(2,1)S(1)} %collective-permute-done.3), channel_id=1, source_target_pairs={{0,1},{1,2},{2,3},{3,4},{4,5},{5,6},{6,7},{7,8},{8,9},{9,10},{10,1... | collective-permute-start | bytes 786440 | tf_op jit(solution)/shard_map/ppermute | solution.py:101
  54.7 6.5 %collective-permute-start.6 = (bf16[1,512,256]{2,1,0:T(8,128)(2,1)S(1)}, bf16[1,512,256]{2,1,0:T(8,128)(2,1)S(1)}, u32[]{:S(2)}, u32[]{:S(2)}) collective-permute-start(bf16[1,512,256]{2,1,0:T(8,128)(2,1)S(1)} %collective-permute-done.4), channel_id=1, source_target_pairs={{0,15},{1,0},{2,1},{3,2},{4,3},{5,4},{6,5},{7,6},{8,7},{9,8},{10,9... | collective-permute-start | bytes 786440 | tf_op jit(solution)/shard_map/ppermute | solution.py:106
  57.8 5.8 %collective-permute-start.7 = (bf16[1,512,256]{2,1,0:T(8,128)(2,1)S(1)}, bf16[1,512,256]{2,1,0:T(8,128)(2,1)S(1)}, u32[]{:S(2)}, u32[]{:S(2)}) collective-permute-start(bf16[1,512,256]{2,1,0:T(8,128)(2,1)S(1)} %collective-permute-done.5), channel_id=1, source_target_pairs={{0,1},{1,2},{2,3},{3,4},{4,5},{5,6},{6,7},{7,8},{8,9},{9,10},{10,1... | collective-permute-start | bytes 786440 | tf_op jit(solution)/shard_map/ppermute | solution.py:101
  61.2 6.7 %collective-permute-start.8 = (bf16[1,512,256]{2,1,0:T(8,128)(2,1)S(1)}, bf16[1,512,256]{2,1,0:T(8,128)(2,1)S(1)}, u32[]{:S(2)}, u32[]{:S(2)}) collective-permute-start(bf16[1,512,256]{2,1,0:T(8,128)(2,1)S(1)} %collective-permute-done.6), channel_id=1, source_target_pairs={{0,15},{1,0},{2,1},{3,2},{4,3},{5,4},{6,5},{7,6},{8,7},{9,8},{10,9... | collective-permute-start | bytes 786440 | tf_op jit(solution)/shard_map/ppermute | solution.py:106
  63.6 5.8 %collective-permute-start.9 = (bf16[1,512,256]{2,1,0:T(8,128)(2,1)S(1)}, bf16[1,512,256]{2,1,0:T(8,128)(2,1)S(1)}, u32[]{:S(2)}, u32[]{:S(2)}) collective-permute-start(bf16[1,512,256]{2,1,0:T(8,128)(2,1)S(1)} %collective-permute-done.7), channel_id=1, source_target_pairs={{0,1},{1,2},{2,3},{3,4},{4,5},{5,6},{6,7},{7,8},{8,9},{9,10},{10,1... | collective-permute-start | bytes 786440 | tf_op jit(solution)/shard_map/ppermute | solution.py:101
  67.9 7.0 %collective-permute-start.10 = (bf16[1,512,256]{2,1,0:T(8,128)(2,1)S(1)}, bf16[1,512,256]{2,1,0:T(8,128)(2,1)S(1)}, u32[]{:S(2)}, u32[]{:S(2)}) collective-permute-start(bf16[1,512,256]{2,1,0:T(8,128)(2,1)S(1)} %collective-permute-done.8), channel_id=1, source_target_pairs={{0,15},{1,0},{2,1},{3,2},{4,3},{5,4},{6,5},{7,6},{8,7},{9,8},{10,9... | collective-permute-start | bytes 786440 | tf_op jit(solution)/shard_map/ppermute | solution.py:106
  69.4 6.4 %collective-permute-start.11 = (bf16[1,512,256]{2,1,0:T(8,128)(2,1)S(1)}, bf16[1,512,256]{2,1,0:T(8,128)(2,1)S(1)}, u32[]{:S(2)}, u32[]{:S(2)}) collective-permute-start(bf16[1,512,256]{2,1,0:T(8,128)(2,1)S(1)} %collective-permute-done.9), channel_id=1, source_target_pairs={{0,1},{1,2},{2,3},{3,4},{4,5},{5,6},{6,7},{7,8},{8,9},{9,10},{10,1... | collective-permute-start | bytes 786440 | tf_op jit(solution)/shard_map/ppermute | solution.py:101
  74.7 16.1 %copy-start.3 = (bf16[1,4096,128]{2,1,0:T(8,128)(2,1)S(1)}, bf16[1,4096,128]{2,1,0:T(8,128)(2,1)}, u32[]{:S(2)}) copy-start(bf16[1,4096,128]{2,1,0:T(8,128)(2,1)} %param.15) | copy-start | bytes 3145732
  74.7 16.1 %copy-start.5 = (f32[4096]{0:T(1024)S(1)}, f32[4096]{0:T(1024)}, u32[]{:S(2)}) copy-start(f32[4096]{0:T(1024)} %param.14) | copy-start | bytes 49156
  74.9 7.0 %collective-permute-start.12 = (bf16[1,512,256]{2,1,0:T(8,128)(2,1)S(1)}, bf16[1,512,256]{2,1,0:T(8,128)(2,1)S(1)}, u32[]{:S(2)}, u32[]{:S(2)}) collective-permute-start(bf16[1,512,256]{2,1,0:T(8,128)(2,1)S(1)} %collective-permute-done.10), channel_id=1, source_target_pairs={{0,15},{1,0},{2,1},{3,2},{4,3},{5,4},{6,5},{7,6},{8,7},{9,8},{10,9... | collective-permute-start | bytes 786440 | tf_op jit(solution)/shard_map/ppermute | solution.py:106
  75.8 7.0 %collective-permute-start.13 = (bf16[1,512,256]{2,1,0:T(8,128)(2,1)S(1)}, bf16[1,512,256]{2,1,0:T(8,128)(2,1)S(1)}, u32[]{:S(2)}, u32[]{:S(2)}) collective-permute-start(bf16[1,512,256]{2,1,0:T(8,128)(2,1)S(1)} %collective-permute-done.11), channel_id=1, source_target_pairs={{0,1},{1,2},{2,3},{3,4},{4,5},{5,6},{6,7},{7,8},{8,9},{9,10},{10,1... | collective-permute-start | bytes 786440 | tf_op jit(solution)/shard_map/ppermute | solution.py:101
  81.9 7.0 %collective-permute-start.14 = (bf16[1,512,256]{2,1,0:T(8,128)(2,1)S(1)}, bf16[1,512,256]{2,1,0:T(8,128)(2,1)S(1)}, u32[]{:S(2)}, u32[]{:S(2)}) collective-permute-start(bf16[1,512,256]{2,1,0:T(8,128)(2,1)S(1)} %collective-permute-done.12), channel_id=1, source_target_pairs={{0,15},{1,0},{2,1},{3,2},{4,3},{5,4},{6,5},{7,6},{8,7},{9,8},{10,9... | collective-permute-start | bytes 786440 | tf_op jit(solution)/shard_map/ppermute | solution.py:106
  82.8 7.0 %collective-permute-start.15 = (bf16[1,512,256]{2,1,0:T(8,128)(2,1)S(1)}, bf16[1,512,256]{2,1,0:T(8,128)(2,1)S(1)}, u32[]{:S(2)}, u32[]{:S(2)}) collective-permute-start(bf16[1,512,256]{2,1,0:T(8,128)(2,1)S(1)} %collective-permute-done.13), channel_id=1, source_target_pairs={{0,1},{1,2},{2,3},{3,4},{4,5},{5,6},{6,7},{7,8},{8,9},{9,10},{10,1... | collective-permute-start | bytes 786440 | tf_op jit(solution)/shard_map/ppermute | solution.py:101
  90.7 1.3 copy-start.4
  93.3 16.0 %copy-start.1 = (bf16[512,128]{1,0:T(8,128)(2,1)S(1)}, bf16[512,128]{1,0:T(8,128)(2,1)}, u32[]{:S(2)}) copy-start(bf16[512,128]{1,0:T(8,128)(2,1)} %param.9) | copy-start | bytes 393220
  95.0 15.7 %copy-start.2 = (f32[128,2]{0,1:T(2,128)S(1)}, f32[128,2]{0,1:T(2,128)}, u32[]{:S(2)}) copy-start(f32[128,2]{0,1:T(2,128)} %param.13) | copy-start | bytes 3076
  95.0 68.4 %all-to-all-start.1 = ((bf16[16,1,512,128]{2,3,1,0:T(8,128)(2,1)}), bf16[16,1,512,128]{2,3,1,0:T(8,128)(2,1)S(1)}, u32[]{:S(2)}, u32[]{:S(2)}) async-start(bf16[16,1,512,128]{2,3,1,0:T(8,128)(2,1)} %broadcast_in_dim.171), calls=%async_computation.1 | async-start | bytes 4194304 | tf_op jit(solution)/shard_map/all_to_all | solution.py:26
  109.1 66.5 %all-gather.2.cloned.1.call-start = ((), (), s32[]{:S(2)}) async-start(), calls=%async_computation.3 | async-start | bytes 2228224 | tf_op jit(solution)/shard_map/all_gather | solution.py:77
  168.1 18.4 %all-to-all-start.2 = ((bf16[32,2,2048]{2,1,0:T(2,128)(2,1)}), bf16[32,2,2048]{2,1,0:T(2,128)(2,1)S(1)}, u32[]{:S(2)}, u32[]{:S(2)}) async-start(bf16[32,2,2048]{2,1,0:T(2,128)(2,1)} %reshape.278), calls=%async_computation.2 | async-start | bytes 524288 | tf_op jit(solution)/shard_map/all_to_all | solution.py:123
Sparse Core Ops, SparseCore 0:
  112.5 63.0 all-gather.1
